TPU v7x, 32 devices: a whole 2x2x4 slice. The times are simulated.
32 devices in a mesh: sp: 8 (over z, x), tp: 4 (over y, core).
Axes of the slice: x: 2, y: 2, z: 4, core: 2. Of those that a mesh axis runs over, the one named last changes fastest.
Arguments:
- residual: bfloat16 [4096, 2048], P('sp'), may hold values from -80 to 80
- queries: bfloat16 [4096, 1024], P('sp', 'tp'), may hold values from -260 to 260
- keys: bfloat16 [4096, 512], P('sp', 'tp'), may hold values from -7 to 7
- values: bfloat16 [4096, 512], P('sp', 'tp'), may hold values from -12 to 12
- documents: int32 [4096], P('sp'), may hold values from 0 to 3, never falling along the last dimension, each value on 1 to 3072 neighbouring positions
- sinks: float32 [16], P('tp'), may hold values from 1 to 6
- out_weight: bfloat16 [1024, 2048], P('tp'), may hold values from -0.5 to 0.5
- norm_gain: float32 [2048], replicated, may hold values from 0.1 to 1.9
- gate_weight: bfloat16 [2048, 5632], P('sp', 'tp'), may hold values from -0.125 to 0.125
- up_weight: bfloat16 [2048, 5632], P('sp', 'tp'), may hold values from -0.125 to 0.125
- down_weight: bfloat16 [2048, 5632], P('sp', 'tp'), may hold values from -0.078125 to 0.078125
Outputs:
- mixed: bfloat16 [4096, 2048], P('sp', 'tp')
Inputs may be any that keep to these rules, and one draw needn't show every extreme that they name: `documents`: document numbers never fall along the positions; a document holds at most 3072 positions.
All inputs are finite; a program needn't handle non-finite values.
Results may differ from a plain program's by a relative error of at most 0.01.
Values may be sent and summed in bfloat16 or wider, within the bound.
A program may use at most 64 MiB of HBM per device.

v0:
```python
import jax
import jax.numpy as jnp
from jax import lax
from jax.sharding import PartitionSpec as P

HEAD_DIM = 64
WINDOW = 128
GROUP = 2
neg_big = -1e30
norm_eps = 1e-05


def from_behind(shard, axis, by):
    length = lax.axis_size(axis)
    pairs = [(i, i + by) for i in range(length) if 0 <= i + by < length]
    return lax.ppermute(shard, axis, pairs)


def attend(queries, keys, values, documents, sinks, tail_keys, tail_values, tail_docs, offset):
    rows_here = queries.shape[0]
    block_count = rows_here // WINDOW
    kv_here = keys.shape[1] // HEAD_DIM
    q_blocks = queries.reshape(block_count, WINDOW, kv_here, GROUP, HEAD_DIM)
    k_blocks = keys.reshape(block_count, WINDOW, kv_here, HEAD_DIM)
    v_blocks = values.reshape(block_count, WINDOW, kv_here, HEAD_DIM)
    k_prev = jnp.concatenate(
        [tail_keys.reshape(1, WINDOW, kv_here, HEAD_DIM), k_blocks[:-1]], axis=0
    )
    v_prev = jnp.concatenate(
        [tail_values.reshape(1, WINDOW, kv_here, HEAD_DIM), v_blocks[:-1]], axis=0
    )
    k_band = jnp.concatenate([k_prev, k_blocks], axis=1)
    v_band = jnp.concatenate([v_prev, v_blocks], axis=1)
    doc_own = documents.astype(jnp.float32).reshape(block_count, WINDOW)
    doc_prev = jnp.concatenate(
        [tail_docs.astype(jnp.float32).reshape(1, WINDOW), doc_own[:-1]], axis=0
    )
    doc_band = jnp.concatenate([doc_prev, doc_own], axis=1)
    row_idx = jnp.arange(WINDOW, dtype=jnp.int32)
    col_idx = jnp.arange(2 * WINDOW, dtype=jnp.int32)
    first = offset + jnp.arange(block_count, dtype=jnp.int32) * WINDOW
    q_pos = first[:, None] + row_idx[None, :]
    k_pos = first[:, None] - WINDOW + col_idx[None, :]
    distance = q_pos[:, :, None] - k_pos[:, None, :]
    visible = (
        (distance >= 0)
        & (distance < WINDOW)
        & (k_pos[:, None, :] >= 0)
        & (doc_own[:, :, None] == doc_band[:, None, :])
    )
    scores = jnp.einsum(
        "nikgd,njkd->nkgij", q_blocks, k_band, preferred_element_type=jnp.float32
    ) * HEAD_DIM ** (-0.5)
    scores = jnp.where(visible[:, None, None], scores, neg_big)
    sink_logit = sinks.reshape(1, kv_here, GROUP, 1, 1)
    row_max = jnp.maximum(scores.max(-1, keepdims=True), sink_logit)
    expo = jnp.where(visible[:, None, None], jnp.exp(scores - row_max), 0.0)
    denom_sum = expo.sum(-1, keepdims=True) + jnp.exp(sink_logit - row_max)
    weights = (expo / denom_sum).astype(jnp.bfloat16)
    mixed = jnp.einsum("nkgij,njkd->nikgd", weights, v_band, preferred_element_type=jnp.float32)
    return mixed.reshape(rows_here, kv_here * GROUP * HEAD_DIM).astype(jnp.bfloat16)


def on_device(
    residual,
    queries,
    keys,
    values,
    documents,
    sinks,
    out_weight,
    norm_gain,
    gate_weight,
    up_weight,
    down_weight,
):
    rows_here = queries.shape[0]
    offset = lax.axis_index("sp") * rows_here
    doc_tail = documents[rows_here - WINDOW :].astype(jnp.bfloat16)
    tail_keys, tail_values, tail_docs = from_behind(
        (keys[rows_here - WINDOW :], values[rows_here - WINDOW :], doc_tail), "sp", 1
    )
    attended = attend(
        queries, keys, values, documents, sinks, tail_keys, tail_values, tail_docs, offset
    )
    model_width = residual.shape[1]
    col_count = model_width // lax.axis_size("tp")
    col_first = lax.axis_index("tp") * col_count
    full_term = jnp.dot(attended, out_weight, preferred_element_type=jnp.float32)
    projected = lax.psum(full_term.astype(jnp.bfloat16), "tp").astype(jnp.float32)
    after_full = (residual.astype(jnp.float32) + projected).astype(jnp.bfloat16)
    after_f = after_full.astype(jnp.float32)
    inv_rms = lax.rsqrt(jnp.mean(after_f * after_f, axis=1, keepdims=True) + norm_eps)
    normed = (after_f * inv_rms * norm_gain[None, :]).astype(jnp.bfloat16)
    after = lax.dynamic_slice_in_dim(after_full, col_first, col_count, 1)
    gate_act = jnp.dot(
        normed,
        lax.all_gather(gate_weight, "sp", axis=0, tiled=True),
        preferred_element_type=jnp.float32,
    )
    up_act = jnp.dot(
        normed,
        lax.all_gather(up_weight, "sp", axis=0, tiled=True),
        preferred_element_type=jnp.float32,
    )
    down_full = lax.all_gather(down_weight, "sp", axis=0, tiled=True)
    hidden = (jax.nn.silu(gate_act) * up_act).astype(jnp.bfloat16)
    summed = lax.psum_scatter(
        lax.dot_general(
            down_full, hidden, (((1,), (1,)), ((), ())), preferred_element_type=jnp.float32
        ).astype(jnp.bfloat16),
        "tp",
        scatter_dimension=0,
        tiled=True,
    ).astype(jnp.float32)
    return (after.astype(jnp.float32) + summed.T).astype(jnp.bfloat16)


def solution(mesh):
    return jax.shard_map(
        on_device,
        mesh=mesh,
        in_specs=(
            P("sp", None),
            P("sp", "tp"),
            P("sp", "tp"),
            P("sp", "tp"),
            P("sp"),
            P("tp"),
            P("tp", None),
            P(),
            P("sp", "tp"),
            P("sp", "tp"),
            P("sp", "tp"),
        ),
        out_specs=P("sp", "tp"),
        check_vma=False,
    )
```

profile of v0, /device:TPU:0, one launch (start us, length us, event | category | flops | bytes accessed | tf_op | source)
XLA Modules:
  0.0 367.5 jit_solution(8054649888373592953)
XLA Ops:
  7.4 0.0 all-reduce.2.cloned.1.call-start
  7.4 0.8 fusion.34
  8.2 4.9 %collective-permute-start.1 = (bf16[128]{0:T(256)(128)(2,1)S(1)}, bf16[128]{0:T(256)(128)(2,1)S(1)}, u32[]{:S(2)}, u32[]{:S(2)}) collective-permute-start(bf16[128]{0:T(256)(128)(2,1)S(1)} %slice.39), channel_id=1, source_target_pairs={{0,4},{4,8},{8,12},{12,16},{16,20},{20,24},{24,28},{1,5},{5,9},{9,... | collective-permute-start | bytes 776 | tf_op jit(solution)/shard_map/ppermute | solution.py:16
  13.1 0.8 slice.42
  13.9 3.4 collective-permute-start.2
  17.3 1.4 slice.36
  18.7 4.0 %collective-permute-start = (bf16[128,128]{1,0:T(8,128)(2,1)}, bf16[128,128]{1,0:T(8,128)(2,1)}, u32[]{:S(2)}, u32[]{:S(2)}) collective-permute-start(bf16[128,128]{1,0:T(8,128)(2,1)} %slice.36), channel_id=1, source_target_pairs={{0,4},{4,8},{8,12},{12,16},{16,20},{20,24},{24,28},{1,5},{5,9},{9,... | collective-permute-start | bytes 98312 | tf_op jit(solution)/shard_map/ppermute | solution.py:16
  22.7 0.1 iota_add_fusion
  22.7 0.1 broadcast_compare_fusion
  22.8 1.0 reshape.148
  23.9 1.0 reshape.146
  24.9 0.1 iota_add_fusion.1
  25.0 2.0 reshape.149
  27.0 0.1 reshape.147
  27.1 0.8 copy.23
  27.9 0.1 copy.25
  28.1 0.1 max.18
  28.2 0.1 reshape.145
  28.3 0.8 copy.18
  29.1 0.1 copy.20
  29.2 0.6 fusion.17
  29.8 0.7 copy.21
  30.5 1.6 fusion.5
  32.2 0.1 broadcast_maximum_fusion
  32.3 0.5 fusion.6
  32.8 0.1 exponential_add_fusion
  32.9 0.9 copy.16
  33.8 0.7 fusion.7
  34.5 0.2 copy.29
  34.7 2.1 convolution_convert_fusion
  36.8 0.0 all-reduce.2.cloned.1.call-update
  36.8 0.0 all-gather.4.cloned.1.call-start
  36.9 0.5 all-gather.4.cloned.1.call-update
  37.4 0.0 all-gather.6.cloned.1.call-start
  37.4 0.5 all-gather.6.cloned.1.call-update
  38.0 0.0 all-gather.8.cloned.1.call-start
  38.0 0.5 all-gather.8.cloned.1.call-update
  38.6 0.2 reduce-scatter.2.cloned.1.call-start
  38.8 48.3 %all-reduce.2.cloned.1.call-done = bf16[512,2048]{1,0:T(8,128)(2,1)} async-done(((bf16[512,2048]{1,0:T(8,128)(2,1)}), bf16[512,2048]{1,0:T(8,128)(2,1)}) %all-reduce.2.cloned.1.call-update) | async-done | bytes 2097168 | tf_op jit(solution)/shard_map/psum | solution.py:90
  87.1 3.2 fusion
  90.3 40.1 %all-gather.4.cloned.1.call-done = bf16[2048,1408]{1,0:T(8,128)(2,1)} async-done(((bf16[256,1408]{1,0:T(8,128)(2,1)}), bf16[2048,1408]{1,0:T(8,128)(2,1)}) %all-gather.4.cloned.1.call-update) | async-done | bytes 5767184 | tf_op jit(solution)/shard_map/all_gather | solution.py:98
  130.4 7.6 %fusion.11 = f32[512,1408]{1,0:T(8,128)} fusion(bf16[2048,1408]{1,0:T(8,128)(2,1)} %all-gather.4.cloned.1.call-done, bf16[512,2048]{1,0:T(8,128)(2,1)S(1)} %get-tuple-element.6, f32[2048]{0:T(1024)S(1)} %copy-done.2, f32[512]{0:T(512)S(1)} %add_rsqrt_fusion), kind=kOutput, calls=%fused_computation.22 | convolution fusion | flops 2956984320 | bytes 10758144 | tf_op jit(solution)/shard_map/dot_general | solution.py:96
  138.0 84.7 %all-gather.6.cloned.1.call-done = bf16[2048,1408]{1,0:T(8,128)(2,1)} async-done(((bf16[256,1408]{1,0:T(8,128)(2,1)}), bf16[2048,1408]{1,0:T(8,128)(2,1)}) %all-gather.6.cloned.1.call-update) | async-done | bytes 5767184 | tf_op jit(solution)/shard_map/all_gather | solution.py:103
  222.7 92.4 %all-gather.8.cloned.1.call-done = bf16[2048,1408]{1,0:T(8,128)(2,1)} async-done(((bf16[256,1408]{1,0:T(8,128)(2,1)}), bf16[2048,1408]{1,0:T(8,128)(2,1)}) %all-gather.8.cloned.1.call-update) | async-done | bytes 5767184 | tf_op jit(solution)/shard_map/all_gather | solution.py:106
  315.1 13.4 %fusion.4 = bf16[2048,512]{0,1:T(8,128)(2,1)} fusion(bf16[2048,1408]{1,0:T(8,128)(2,1)} %all-gather.8.cloned.1.call-done, bf16[2048,1408]{1,0:T(8,128)(2,1)} %all-gather.6.cloned.1.call-done, f32[512,1408]{1,0:T(8,128)} %fusion.11, bf16[512,2048]{1,0:T(8,128)(2,1)S(1)} %get-tuple-element.6, f32[2048]{0:T(1024)S(1)} %copy-done.2, f32[512]{0:T(512)S(1)} %add_rsqrt_fusion), kind=kOutput, calls=%fused_computation.10 | convolution fusion | flops 5915148288 | bytes 18622464 | tf_op jit(solution)/shard_map/dot_general | solution.py:109
  328.5 0.0 reduce-scatter.2.cloned.1.call-update
  328.5 29.5 %reduce-scatter.2.cloned.1.call-done = bf16[512,512]{0,1:T(8,128)(2,1)} async-done(((bf16[2048,512]{0,1:T(8,128)(2,1)}), bf16[512,512]{0,1:T(8,128)(2,1)}) %reduce-scatter.2.cloned.1.call-update) | async-done | bytes 524304 | tf_op jit(solution)/shard_map/reduce_scatter | solution.py:108
  358.0 2.0 fusion.8
  (21 shorter events, 0.1 us)
Async XLA Ops:
  7.4 27.3 %copy-start = (bf16[256,2048]{1,0:T(8,128)(2,1)S(1)}, bf16[256,2048]{1,0:T(8,128)(2,1)}, u32[]{:S(2)}) copy-start(bf16[256,2048]{1,0:T(8,128)(2,1)} %param.17) | copy-start | bytes 3145732
  7.4 19.6 %slice-start = ((bf16[512,128]{1,0:T(8,128)(2,1)}), bf16[384,128]{1,0:T(8,128)(2,1)S(1)}, s32[]{:S(2)}) async-start(bf16[512,128]{1,0:T(8,128)(2,1)} %param.13), calls=%async_computation.6 | async-start | bytes 196608 | tf_op jit(solution)/shard_map/slice | solution.py:27
  7.4 20.8 %slice-start.1 = ((bf16[512,128]{1,0:T(8,128)(2,1)}), bf16[384,128]{1,0:T(8,128)(2,1)S(1)}, s32[]{:S(2)}) async-start(bf16[512,128]{1,0:T(8,128)(2,1)} %param.14), calls=%async_computation.7 | async-start | bytes 196608 | tf_op jit(solution)/shard_map/slice | solution.py:30
  7.4 20.7 %copy-start.3 = (f32[4]{0:T(128)S(1)}, f32[4]{0:T(128)}, u32[]{:S(2)}) copy-start(f32[4]{0:T(128)} %param.16) | copy-start | bytes 52
  7.4 79.7 %all-reduce.2.cloned.1.call-start = ((), (), s32[]{:S(2)}) async-start(), calls=%async_computation.1 | async-start | bytes 4194304 | tf_op jit(solution)/shard_map/psum | solution.py:90
  8.2 21.0 %collective-permute-start.1 = (bf16[128]{0:T(256)(128)(2,1)S(1)}, bf16[128]{0:T(256)(128)(2,1)S(1)}, u32[]{:S(2)}, u32[]{:S(2)}) collective-permute-start(bf16[128]{0:T(256)(128)(2,1)S(1)} %slice.39), channel_id=1, source_target_pairs={{0,4},{4,8},{8,12},{12,16},{16,20},{20,24},{24,28},{1,5},{5,9},{9,... | collective-permute-start | bytes 776 | tf_op jit(solution)/shard_map/ppermute | solution.py:16
  13.9 16.0 %collective-permute-start.2 = (bf16[128,128]{1,0:T(8,128)(2,1)S(1)}, bf16[128,128]{1,0:T(8,128)(2,1)S(1)}, u32[]{:S(2)}, u32[]{:S(2)}) collective-permute-start(bf16[128,128]{1,0:T(8,128)(2,1)S(1)} %slice.42), channel_id=1, source_target_pairs={{0,4},{4,8},{8,12},{12,16},{16,20},{20,24},{24,28},{1,5},{5,9},{9,... | collective-permute-start | bytes 98312 | tf_op jit(solution)/shard_map/ppermute | solution.py:16
  18.7 14.2 %collective-permute-start = (bf16[128,128]{1,0:T(8,128)(2,1)}, bf16[128,128]{1,0:T(8,128)(2,1)}, u32[]{:S(2)}, u32[]{:S(2)}) collective-permute-start(bf16[128,128]{1,0:T(8,128)(2,1)} %slice.36), channel_id=1, source_target_pairs={{0,4},{4,8},{8,12},{12,16},{16,20},{20,24},{24,28},{1,5},{5,9},{9,... | collective-permute-start | bytes 98312 | tf_op jit(solution)/shard_map/ppermute | solution.py:16
  32.2 1.6 copy-start.1
  36.8 93.5 %all-gather.4.cloned.1.call-start = ((), (), s32[]{:S(2)}) async-start(), calls=%async_computation.2 | async-start | bytes 6488064 | tf_op jit(solution)/shard_map/all_gather | solution.py:98
  37.4 185.3 %all-gather.6.cloned.1.call-start = ((), (), s32[]{:S(2)}) async-start(), calls=%async_computation.3 | async-start | bytes 6488064 | tf_op jit(solution)/shard_map/all_gather | solution.py:103
  38.0 277.1 %all-gather.8.cloned.1.call-start = ((), (), s32[]{:S(2)}) async-start(), calls=%async_computation.4 | async-start | bytes 6488064 | tf_op jit(solution)/shard_map/all_gather | solution.py:106
  38.6 91.8 %copy-start.2 = (f32[2048]{0:T(1024)S(1)}, f32[2048]{0:T(1024)}, u32[]{:S(2)}) copy-start(f32[2048]{0:T(1024)} %param.18) | copy-start | bytes 24580
  38.6 319.4 %reduce-scatter.2.cloned.1.call-start = ((), (), s32[]{:S(2)}) async-start(), calls=%async_computation.5 | async-start | bytes 2621440 | tf_op jit(solution)/shard_map/reduce_scatter | solution.py:108
Sparse Core Ops, SparseCore 0:
  36.9 50.1 all-reduce.1
  328.6 29.2 reduce-scatter.1
Sparse Core Ops, SparseCore 1:
  39.5 90.8 all-gather.3
  132.4 90.2 all-gather.5
  224.8 90.2 all-gather.7
where the time goes:
time: 368 us
  waiting for transfers between devices  296 us (80%)
  matrix products  25.5 us (7%)
  between operations  15.2 us (4%)
  starting transfers between devices  12.7 us (3%)
  local copies, waits for them, and re-layouts  10.2 us (3%)
  other arithmetic  7.52 us (2%)
    all_gather x1, waiting for transfers between devices, on_device(): down_full = lax.all_gather(down_weight, 'sp', axis=0, tiled=True)  92.4 us
    all_gather x1, waiting for transfers between devices, on_device(): lax.all_gather(up_weight, 'sp', axis=0, tiled=True)  84.7 us
    psum x1, waiting for transfers between devices, on_device(): lax.psum(full_term.astype(jnp.bfloat16), 'tp').astype(jnp.float32)  48.3 us
    all_gather x1, waiting for transfers between devices, on_device(): lax.all_gather(gate_weight, 'sp', axis=0, tiled=True)  40.1 us
    reduce_scatter x1, waiting for transfers between devices, on_device(): lax.psum_scatter(lax.dot_general(down_full, hidden, (((1,), (1,)), ((), (...  29.5 us
    dot_general x1, matrix products, on_device(): lax.dot_general(down_full, hidden, (((1,), (1,)), ((), ())), preferred_el...  13.4 us
    ppermute x3, starting transfers between devices, from_behind(): return lax.ppermute(shard, axis, pairs)  12.3 us
    dot_general x1, matrix products, on_device(): jnp.dot(normed, lax.all_gather(gate_weight, 'sp', axis=0, tiled=True), pr...  7.64 us
  transfers between devices with their start and end apart: 8, of which 5 were waited for; matrix products, arithmetic and copies ran while one was open for 6% of the time, Pallas kernels for 0%

commit v1 on v0

--- a/solution.py
+++ b/solution.py
@@ -8,6 +8,16 @@
 GROUP = 2
 neg_big = -1e30
 norm_eps = 1e-05
+
+
+def gather_by_hops(x, name, dim):
+    size = lax.axis_size(name)
+    held, parts = (x, [x])
+    for _ in range(size - 1):
+        held = lax.ppermute(held, name, [(i, (i + 1) % size) for i in range(size)])
+        parts.insert(0, held)
+    line = jnp.concatenate(parts, axis=dim)
+    return jnp.roll(line, (lax.axis_index(name) + 1) * x.shape[dim], axis=dim)
 
 
 def from_behind(shard, axis, by):
@@ -103,7 +113,7 @@
         lax.all_gather(up_weight, "sp", axis=0, tiled=True),
         preferred_element_type=jnp.float32,
     )
-    down_full = lax.all_gather(down_weight, "sp", axis=0, tiled=True)
+    down_full = gather_by_hops(down_weight, "sp", 0)
     hidden = (jax.nn.silu(gate_act) * up_act).astype(jnp.bfloat16)
     summed = lax.psum_scatter(
         lax.dot_general(

time: 368 us -> 357 us (0.970)
  waiting for transfers between devices: 296 us -> 257 us
  local copies, waits for them, and re-layouts: 10.2 us -> 36.5 us
    ppermute x0 -> x7, waiting for transfers between devices: none -> 209 us  [gather_by_hops(): held = lax.ppermute(held, name, [(i, (i + 1) % size) for i in range(size)])]
    all_gather x1 -> x0, waiting for transfers between devices: 92.4 us -> none  [on_device(): down_full = lax.all_gather(down_weight, 'sp', axis=0, tiled=True)]
    all_gather x1, waiting for transfers between devices: 84.7 us -> 16.2 us  [on_device(): lax.all_gather(up_weight, 'sp', axis=0, tiled=True)]
    psum x1, waiting for transfers between devices: 48.3 us -> 0.01 us  [on_device(): lax.psum(full_term.astype(jnp.bfloat16), 'tp').astype(jnp.float32)]
    all_gather x1, waiting for transfers between devices: 40.1 us -> 0.01 us  [on_device(): lax.all_gather(gate_weight, 'sp', axis=0, tiled=True)]
    unnamed x8 -> x43, local copies, waits for them, and re-layouts: 0.02 us -> 22.9 us
  transfers between devices with their start and end apart: 8 -> 14, of which waited for: 5 -> 9; matrix products, arithmetic and copies ran while one was open for 6% -> 13% of each run, Pallas kernels for 0% -> 0%
where the time goes in v1:
time: 357 us; the launch traced here: 356 us
  waiting for transfers between devices  257 us (72%)
  local copies, waits for them, and re-layouts  36.5 us (10%)
  matrix products  26.3 us (7%)
  between operations  15.1 us (4%)
  starting transfers between devices  13.4 us (4%)
  other arithmetic  7.62 us (2%)
    ppermute x7, waiting for transfers between devices, gather_by_hops(): held = lax.ppermute(held, name, [(i, (i + 1) % size) for i in range(size)])  209 us
    reduce_scatter x1, waiting for transfers between devices, on_device(): lax.psum_scatter(lax.dot_general(down_full, hidden, (((1,), (1,)), ((), (...  30.9 us
    unnamed x43, local copies, waits for them, and re-layouts  22.9 us
    all_gather x1, waiting for transfers between devices, on_device(): lax.all_gather(up_weight, 'sp', axis=0, tiled=True)  16.2 us
    dot_general x1, matrix products, on_device(): lax.dot_general(down_full, hidden, (((1,), (1,)), ((), ())), preferred_el...  13.3 us
    ppermute x3, starting transfers between devices, from_behind(): return lax.ppermute(shard, axis, pairs)  12.3 us
    dot_general x1, matrix products, on_device(): jnp.dot(normed, lax.all_gather(gate_weight, 'sp', axis=0, tiled=True), pr...  7.77 us
  transfers between devices with their start and end apart: 14, of which 9 were waited for; matrix products, arithmetic and copies ran while one was open for 13% of the time, Pallas kernels for 0%

profile of v1, /device:TPU:0, one launch (start us, length us, event | category | flops | bytes accessed | tf_op | source)
XLA Modules:
  0.0 355.8 jit_solution(9829766244546412125)
XLA Ops:
  8.2 4.9 %collective-permute-start.1 = (bf16[128]{0:T(256)(128)(2,1)S(1)}, bf16[128]{0:T(256)(128)(2,1)S(1)}, u32[]{:S(2)}, u32[]{:S(2)}) collective-permute-start(bf16[128]{0:T(256)(128)(2,1)S(1)} %slice.39), channel_id=1, source_target_pairs={{0,4},{4,8},{8,12},{12,16},{16,20},{20,24},{24,28},{1,5},{5,9},{9,... | collective-permute-start | bytes 776 | tf_op jit(solution)/shard_map/ppermute | solution.py:26
  13.8 3.4 collective-permute-start.2
  17.3 1.4 slice.36
  18.6 4.0 %collective-permute-start = (bf16[128,128]{1,0:T(8,128)(2,1)}, bf16[128,128]{1,0:T(8,128)(2,1)}, u32[]{:S(2)}, u32[]{:S(2)}) collective-permute-start(bf16[128,128]{1,0:T(8,128)(2,1)} %slice.36), channel_id=1, source_target_pairs={{0,4},{4,8},{8,12},{12,16},{16,20},{20,24},{24,28},{1,5},{5,9},{9,... | collective-permute-start | bytes 98312 | tf_op jit(solution)/shard_map/ppermute | solution.py:26
  22.8 1.0 reshape.148
  23.8 0.9 slice.43
  24.7 1.0 reshape.146
  25.8 0.9 slice.37
  26.7 2.0 reshape.149
  32.9 1.6 fusion.9
  35.3 0.9 copy.17
  36.1 1.6 fusion.11
  38.0 2.0 convolution_convert_fusion
  41.3 1.0 collective-permute-start.3
  42.3 26.5 %collective-permute-done.3 = bf16[256,1408]{1,0:T(8,128)(2,1)S(1)} collective-permute-done((bf16[256,1408]{1,0:T(8,128)(2,1)S(1)}, bf16[256,1408]{1,0:T(8,128)(2,1)S(1)}, u32[]{:S(2)}, u32[]{:S(2)}) %collective-permute-start.3) | collective-permute-done | bytes 720928 | tf_op jit(solution)/shard_map/ppermute | solution.py:17
  68.8 0.9 copy-done.3
  69.7 30.1 %collective-permute-done.4 = bf16[256,1408]{1,0:T(8,128)(2,1)S(1)} collective-permute-done((bf16[256,1408]{1,0:T(8,128)(2,1)S(1)}, bf16[256,1408]{1,0:T(8,128)(2,1)S(1)}, u32[]{:S(2)}, u32[]{:S(2)}) %collective-permute-start.4) | collective-permute-done | bytes 720928 | tf_op jit(solution)/shard_map/ppermute | solution.py:17
  99.8 0.9 copy-done.5
  100.7 35.4 %collective-permute-done.5 = bf16[256,1408]{1,0:T(8,128)(2,1)S(1)} collective-permute-done((bf16[256,1408]{1,0:T(8,128)(2,1)S(1)}, bf16[256,1408]{1,0:T(8,128)(2,1)S(1)}, u32[]{:S(2)}, u32[]{:S(2)}) %collective-permute-start.5) | collective-permute-done | bytes 720928 | tf_op jit(solution)/shard_map/ppermute | solution.py:17
  136.1 0.8 copy-done.7
  137.0 35.2 %collective-permute-done.6 = bf16[256,1408]{1,0:T(8,128)(2,1)S(1)} collective-permute-done((bf16[256,1408]{1,0:T(8,128)(2,1)S(1)}, bf16[256,1408]{1,0:T(8,128)(2,1)S(1)}, u32[]{:S(2)}, u32[]{:S(2)}) %collective-permute-start.6) | collective-permute-done | bytes 720928 | tf_op jit(solution)/shard_map/ppermute | solution.py:17
  172.1 0.9 copy-done.9
  173.0 23.6 %collective-permute-done.7 = bf16[256,1408]{1,0:T(8,128)(2,1)S(1)} collective-permute-done((bf16[256,1408]{1,0:T(8,128)(2,1)S(1)}, bf16[256,1408]{1,0:T(8,128)(2,1)S(1)}, u32[]{:S(2)}, u32[]{:S(2)}) %collective-permute-start.7) | collective-permute-done | bytes 720928 | tf_op jit(solution)/shard_map/ppermute | solution.py:17
  196.7 0.9 copy-done.11
  197.6 35.2 %collective-permute-done.8 = bf16[256,1408]{1,0:T(8,128)(2,1)} collective-permute-done((bf16[256,1408]{1,0:T(8,128)(2,1)S(1)}, bf16[256,1408]{1,0:T(8,128)(2,1)}, u32[]{:S(2)}, u32[]{:S(2)}) %collective-permute-start.8) | collective-permute-done | bytes 720928 | tf_op jit(solution)/shard_map/ppermute | solution.py:17
  232.7 3.3 fusion.2
  236.1 22.8 %collective-permute-done.9 = bf16[256,1408]{1,0:T(8,128)(2,1)} collective-permute-done((bf16[256,1408]{1,0:T(8,128)(2,1)}, bf16[256,1408]{1,0:T(8,128)(2,1)}, u32[]{:S(2)}, u32[]{:S(2)}) %collective-permute-start.9) | collective-permute-done | bytes 720928 | tf_op jit(solution)/shard_map/ppermute | solution.py:17
  258.9 2.0 constant_dynamic-update-slice_fusion.15
  260.9 2.1 constant_dynamic-update-slice_fusion.14
  263.0 0.9 constant_dynamic-update-slice_fusion.13
  263.9 0.9 constant_dynamic-update-slice_fusion.12
  264.9 0.9 constant_dynamic-update-slice_fusion.11
  265.8 0.9 constant_dynamic-update-slice_fusion.10
  266.7 0.9 constant_dynamic-update-slice_fusion.9
  267.6 0.9 constant_dynamic-update-slice_fusion.8
  268.5 2.0 constant_dynamic-update-slice_fusion.7
  270.6 2.0 constant_dynamic-update-slice_fusion.6
  272.6 0.9 constant_dynamic-update-slice_fusion.5
  273.5 1.0 constant_dynamic-update-slice_fusion.4
  274.5 1.0 constant_dynamic-update-slice_fusion.3
  275.5 0.9 constant_dynamic-update-slice_fusion.2
  276.4 0.9 constant_dynamic-update-slice_fusion.1
  277.3 0.9 constant_dynamic-update-slice_fusion
  278.2 7.8 %fusion.14 = f32[512,1408]{1,0:T(8,128)} fusion(bf16[2048,1408]{1,0:T(8,128)(2,1)} %all-gather.3.cloned.1.call-done, bf16[512,2048]{1,0:T(8,128)(2,1)S(1)} %get-tuple-element.6, f32[2048]{0:T(1024)S(1)} %copy-done.13, f32[512]{0:T(512)S(1)} %add_rsqrt_fusion), kind=kOutput, calls=%fused_computation.23 | convolution fusion | flops 2956984320 | bytes 10758144 | tf_op jit(solution)/shard_map/dot_general | solution.py:106
  286.0 16.2 %all-gather.5.cloned.1.call-done = bf16[2048,1408]{1,0:T(8,128)(2,1)} async-done(((bf16[256,1408]{1,0:T(8,128)(2,1)}), bf16[2048,1408]{1,0:T(8,128)(2,1)}) %all-gather.5.cloned.1.call-update) | async-done | bytes 5767184 | tf_op jit(solution)/shard_map/all_gather | solution.py:113
  302.2 13.3 %fusion.6 = bf16[2048,512]{0,1:T(8,128)(2,1)} fusion(bf16[4096,1408]{1,0:T(8,128)(2,1)} %constant_dynamic-update-slice_fusion, s32[]{:T(128)S(6)} %select_n.27, bf16[2048,1408]{1,0:T(8,128)(2,1)} %all-gather.5.cloned.1.call-done, f32[512,1408]{1,0:T(8,128)} %fusion.14, bf16[512,2048]{1,0:T(8,128)(2,1)S(1)} %get-tuple-element.6, f32[2048]{0:T(1024)S(1)} %copy-done.13, ...), kind=kOutput, calls=%fused_computation.11 | convolution fusion | flops 5915148288 | bytes 18622468 | tf_op jit(solution)/shard_map/dot_general | solution.py:119
  315.5 30.9 %reduce-scatter.2.cloned.1.call-done = bf16[512,512]{0,1:T(8,128)(2,1)} async-done(((bf16[2048,512]{0,1:T(8,128)(2,1)}), bf16[512,512]{0,1:T(8,128)(2,1)}) %reduce-scatter.2.cloned.1.call-update) | async-done | bytes 524304 | tf_op jit(solution)/shard_map/reduce_scatter | solution.py:118
  346.4 2.0 fusion.12
  (66 shorter events, 8.1 us)
Async XLA Ops:
  7.4 30.6 %copy-start = (bf16[256,2048]{1,0:T(8,128)(2,1)S(1)}, bf16[256,2048]{1,0:T(8,128)(2,1)}, u32[]{:S(2)}) copy-start(bf16[256,2048]{1,0:T(8,128)(2,1)} %param.17) | copy-start | bytes 3145732
  7.4 225.4 %all-reduce.2.cloned.1.call-start = ((), (), s32[]{:S(2)}) async-start(), calls=%async_computation.1 | async-start | bytes 4194304 | tf_op jit(solution)/shard_map/psum | solution.py:100
  8.2 23.4 %collective-permute-start.1 = (bf16[128]{0:T(256)(128)(2,1)S(1)}, bf16[128]{0:T(256)(128)(2,1)S(1)}, u32[]{:S(2)}, u32[]{:S(2)}) collective-permute-start(bf16[128]{0:T(256)(128)(2,1)S(1)} %slice.39), channel_id=1, source_target_pairs={{0,4},{4,8},{8,12},{12,16},{16,20},{20,24},{24,28},{1,5},{5,9},{9,... | collective-permute-start | bytes 776 | tf_op jit(solution)/shard_map/ppermute | solution.py:26
  13.8 18.4 %collective-permute-start.2 = (bf16[128,128]{1,0:T(8,128)(2,1)S(1)}, bf16[128,128]{1,0:T(8,128)(2,1)S(1)}, u32[]{:S(2)}, u32[]{:S(2)}) collective-permute-start(bf16[128,128]{1,0:T(8,128)(2,1)S(1)} %slice.42), channel_id=1, source_target_pairs={{0,4},{4,8},{8,12},{12,16},{16,20},{20,24},{24,28},{1,5},{5,9},{9,... | collective-permute-start | bytes 98312 | tf_op jit(solution)/shard_map/ppermute | solution.py:26
  18.6 16.6 %collective-permute-start = (bf16[128,128]{1,0:T(8,128)(2,1)}, bf16[128,128]{1,0:T(8,128)(2,1)}, u32[]{:S(2)}, u32[]{:S(2)}) collective-permute-start(bf16[128,128]{1,0:T(8,128)(2,1)} %slice.36), channel_id=1, source_target_pairs={{0,4},{4,8},{8,12},{12,16},{16,20},{20,24},{24,28},{1,5},{5,9},{9,... | collective-permute-start | bytes 98312 | tf_op jit(solution)/shard_map/ppermute | solution.py:26
  37.7 3.5 copy-start.1
  40.0 238.2 %all-gather.3.cloned.1.call-start = ((), (), s32[]{:S(2)}) async-start(), calls=%async_computation.2 | async-start | bytes 6488064 | tf_op jit(solution)/shard_map/all_gather | solution.py:108
  40.6 261.6 %all-gather.5.cloned.1.call-start = ((), (), s32[]{:S(2)}) async-start(), calls=%async_computation.3 | async-start | bytes 6488064 | tf_op jit(solution)/shard_map/all_gather | solution.py:113
  41.2 305.1 %reduce-scatter.2.cloned.1.call-start = ((), (), s32[]{:S(2)}) async-start(), calls=%async_computation.4 | async-start | bytes 2621440 | tf_op jit(solution)/shard_map/reduce_scatter | solution.py:118
  41.3 27.5 %collective-permute-start.3 = (bf16[256,1408]{1,0:T(8,128)(2,1)S(1)}, bf16[256,1408]{1,0:T(8,128)(2,1)S(1)}, u32[]{:S(2)}, u32[]{:S(2)}) collective-permute-start(bf16[256,1408]{1,0:T(8,128)(2,1)S(1)} %copy-done.1), channel_id=1, source_target_pairs={{0,4},{4,8},{8,12},{12,16},{16,20},{20,24},{24,28},{28,0},{1,5},{5... | collective-permute-start | bytes 2162696 | tf_op jit(solution)/shard_map/ppermute | solution.py:17
  68.8 0.9 copy-start.3
  69.7 30.1 %collective-permute-start.4 = (bf16[256,1408]{1,0:T(8,128)(2,1)S(1)}, bf16[256,1408]{1,0:T(8,128)(2,1)S(1)}, u32[]{:S(2)}, u32[]{:S(2)}) collective-permute-start(bf16[256,1408]{1,0:T(8,128)(2,1)S(1)} %collective-permute-done.3), channel_id=1, source_target_pairs={{0,4},{4,8},{8,12},{12,16},{16,20},{20,24},{24,28},{28,0},{1,5},{5... | collective-permute-start | bytes 2162696 | tf_op jit(solution)/shard_map/ppermute | solution.py:17
  99.8 0.9 copy-start.5
  100.7 35.4 %collective-permute-start.5 = (bf16[256,1408]{1,0:T(8,128)(2,1)S(1)}, bf16[256,1408]{1,0:T(8,128)(2,1)S(1)}, u32[]{:S(2)}, u32[]{:S(2)}) collective-permute-start(bf16[256,1408]{1,0:T(8,128)(2,1)S(1)} %collective-permute-done.4), channel_id=1, source_target_pairs={{0,4},{4,8},{8,12},{12,16},{16,20},{20,24},{24,28},{28,0},{1,5},{5... | collective-permute-start | bytes 2162696 | tf_op jit(solution)/shard_map/ppermute | solution.py:17
  136.1 0.8 copy-start.7
  137.0 35.2 %collective-permute-start.6 = (bf16[256,1408]{1,0:T(8,128)(2,1)S(1)}, bf16[256,1408]{1,0:T(8,128)(2,1)S(1)}, u32[]{:S(2)}, u32[]{:S(2)}) collective-permute-start(bf16[256,1408]{1,0:T(8,128)(2,1)S(1)} %collective-permute-done.5), channel_id=1, source_target_pairs={{0,4},{4,8},{8,12},{12,16},{16,20},{20,24},{24,28},{28,0},{1,5},{5... | collective-permute-start | bytes 2162696 | tf_op jit(solution)/shard_map/ppermute | solution.py:17
  172.1 0.9 copy-start.9
  173.0 23.7 %collective-permute-start.7 = (bf16[256,1408]{1,0:T(8,128)(2,1)S(1)}, bf16[256,1408]{1,0:T(8,128)(2,1)S(1)}, u32[]{:S(2)}, u32[]{:S(2)}) collective-permute-start(bf16[256,1408]{1,0:T(8,128)(2,1)S(1)} %collective-permute-done.6), channel_id=1, source_target_pairs={{0,4},{4,8},{8,12},{12,16},{16,20},{20,24},{24,28},{28,0},{1,5},{5... | collective-permute-start | bytes 2162696 | tf_op jit(solution)/shard_map/ppermute | solution.py:17
  196.7 0.9 copy-start.11
  197.6 35.2 %collective-permute-start.8 = (bf16[256,1408]{1,0:T(8,128)(2,1)S(1)}, bf16[256,1408]{1,0:T(8,128)(2,1)}, u32[]{:S(2)}, u32[]{:S(2)}) collective-permute-start(bf16[256,1408]{1,0:T(8,128)(2,1)S(1)} %collective-permute-done.7), channel_id=1, source_target_pairs={{0,4},{4,8},{8,12},{12,16},{16,20},{20,24},{24,28},{28,0},{1,5},{5... | collective-permute-start | bytes 2162696 | tf_op jit(solution)/shard_map/ppermute | solution.py:17
  232.7 26.1 %collective-permute-start.9 = (bf16[256,1408]{1,0:T(8,128)(2,1)}, bf16[256,1408]{1,0:T(8,128)(2,1)}, u32[]{:S(2)}, u32[]{:S(2)}) collective-permute-start(bf16[256,1408]{1,0:T(8,128)(2,1)} %collective-permute-done.8), channel_id=1, source_target_pairs={{0,4},{4,8},{8,12},{12,16},{16,20},{20,24},{24,28},{28,0},{1,5},{5... | collective-permute-start | bytes 2162696 | tf_op jit(solution)/shard_map/ppermute | solution.py:17
  232.7 30.3 %copy-start.12 = (bf16[256,1408]{1,0:T(8,128)(2,1)S(1)}, bf16[256,1408]{1,0:T(8,128)(2,1)}, u32[]{:S(2)}) copy-start(bf16[256,1408]{1,0:T(8,128)(2,1)} %copy-done.11) | copy-start | bytes 2162692
  232.7 31.2 %copy-start.10 = (bf16[256,1408]{1,0:T(8,128)(2,1)S(1)}, bf16[256,1408]{1,0:T(8,128)(2,1)}, u32[]{:S(2)}) copy-start(bf16[256,1408]{1,0:T(8,128)(2,1)} %copy-done.9) | copy-start | bytes 2162692
  236.1 28.8 %copy-start.8 = (bf16[256,1408]{1,0:T(8,128)(2,1)S(1)}, bf16[256,1408]{1,0:T(8,128)(2,1)}, u32[]{:S(2)}) copy-start(bf16[256,1408]{1,0:T(8,128)(2,1)} %copy-done.7) | copy-start | bytes 2162692
  236.1 29.7 %copy-start.6 = (bf16[256,1408]{1,0:T(8,128)(2,1)S(1)}, bf16[256,1408]{1,0:T(8,128)(2,1)}, u32[]{:S(2)}) copy-start(bf16[256,1408]{1,0:T(8,128)(2,1)} %copy-done.5) | copy-start | bytes 2162692
  236.1 30.6 %copy-start.4 = (bf16[256,1408]{1,0:T(8,128)(2,1)S(1)}, bf16[256,1408]{1,0:T(8,128)(2,1)}, u32[]{:S(2)}) copy-start(bf16[256,1408]{1,0:T(8,128)(2,1)} %copy-done.3) | copy-start | bytes 2162692
  260.9 6.7 %copy-start.2 = (bf16[256,1408]{1,0:T(8,128)(2,1)S(1)}, bf16[256,1408]{1,0:T(8,128)(2,1)}, u32[]{:S(2)}) copy-start(bf16[256,1408]{1,0:T(8,128)(2,1)} %param.21) | copy-start | bytes 2162692
  272.6 5.6 %copy-start.13 = (f32[2048]{0:T(1024)S(1)}, f32[2048]{0:T(1024)}, u32[]{:S(2)}) copy-start(f32[2048]{0:T(1024)} %param.18) | copy-start | bytes 24580
Sparse Core Ops, SparseCore 0:
  40.2 50.0 all-reduce.1
  315.6 30.6 reduce-scatter.1
Sparse Core Ops, SparseCore 1:
  42.7 132.2 all-gather.2
  177.0 125.1 all-gather.4
